TPU v7x, 32 devices: a whole 2x2x4 slice. The times are simulated.
32 devices in a mesh: grp: 2 (over y), sp: 8 (over z, core), tp: 2 (over x).
Axes of the slice: x: 2, y: 2, z: 4, core: 2. Of those that a mesh axis runs over, the one named last changes fastest.
Arguments:
- tokens: bfloat16 [12288, 2048], P(('grp', 'sp'), 'tp'), parts along dimension 0, may hold values from -4000 to 4000
- gain: float32 [2048], replicated, may hold values from 0.1 to 1.9
- w_query: bfloat16 [2048, 1024], P('sp', 'tp'), may hold values from -1 to 1
- w_key: bfloat16 [2048, 256], P('sp', 'tp'), may hold values from -1 to 1
- w_value: bfloat16 [2048, 256], P('sp', 'tp'), may hold values from -0.125 to 0.125
- w_input: bfloat16 [2048, 1024], P('sp', 'tp'), may hold values from -0.125 to 0.125
- w_bgate: bfloat16 [2048, 1024], P('sp', 'tp'), may hold values from -0.125 to 0.125
- w_cgate: bfloat16 [2048, 1024], P('sp', 'tp'), may hold values from -0.125 to 0.125
- w_attn_out: bfloat16 [1024, 2048], P('sp', 'tp'), may hold values from -2 to 2
- w_conv_out: bfloat16 [1024, 2048], P('sp', 'tp'), may hold values from -0.1875 to 0.1875
- sink_logit: float32 [16], P('tp'), may hold values from 0 to 5
- taps: float32 [3, 1024], P(None, 'tp'), may hold values from -3.5 to 3.5
- conv_bias: float32 [1024], P('tp'), may hold values from -4 to 4
- documents: int32 [12288], P(('grp', 'sp')), parts along dimension 0, may hold values from 0 to 3, never falling along the last dimension, each value on 1 to 3072 neighbouring positions
Outputs:
- mixed: bfloat16 [12288, 2048], P(('grp', 'sp'), 'tp'), parts along dimension 0
There are 2 independent parts, one for each index of `grp`. A program takes and returns all parts, laid end to end along the dimension named above; an argument that names none is the same for every part. Nothing has to cross between parts.
All inputs are finite; a program needn't handle non-finite values.
Results may differ from a plain program's by a relative error of at most 0.013.
The roundings to bfloat16 on the way count: a program that leaves them out, or rounds other values in their place, can miss the bound.
Values may be sent and summed in bfloat16 or wider, within the bound.
A program may use at most 64 MiB of HBM per device.

v0:
```python
import jax
import jax.numpy as jnp
from jax import lax
from jax.sharding import PartitionSpec as P

HEAD_DIM = 64
WINDOW = 128
EPS = 1e-06
THETA = 500000.0


def extended(cells, sides, width):
    for axis, dim in sides:
        count = lax.axis_size(axis)
        ends = count - 1
        head = lax.slice_in_dim(cells, 0, width, axis=dim)
        tail = lax.slice_in_dim(cells, cells.shape[dim] - width, cells.shape[dim], axis=dim)
        cells = jnp.concatenate(
            [
                lax.ppermute(tail, axis, [(i, (i + 1) % count) for i in range(ends)]),
                cells,
                lax.ppermute(head, axis, [((i + 1) % count, i) for i in range(ends)]),
            ],
            axis=dim,
        )
    return cells


def rotate(proj, positions, heads):
    rows = proj.shape[0]
    size = proj.shape[1] // heads
    half = size // 2
    freq = jnp.power(THETA, -(jnp.arange(half, dtype=jnp.float32) * (2.0 / size)))
    angle = positions.astype(jnp.float32)[:, None] * freq[None, :]
    cosine = jnp.cos(angle)[:, None, :]
    sine = jnp.sin(angle)[:, None, :]
    shaped = proj.reshape(rows, heads, size)
    first = shaped[..., :half]
    second = shaped[..., half:]
    turned = jnp.concatenate(
        [first * cosine - second * sine, second * cosine + first * sine], axis=-1
    )
    return turned.reshape(rows, heads * size)


def sink_softmax(scores, allowed, sinks):
    masked = jnp.where(allowed, scores, -jnp.inf)
    top = jnp.maximum(jnp.max(masked, axis=-1, keepdims=True), sinks)
    expo = jnp.exp(masked - top)
    return expo / (jnp.sum(expo, axis=-1, keepdims=True) + jnp.exp(sinks - top))


def local(
    tokens,
    gain,
    w_query,
    w_key,
    w_value,
    w_input,
    w_bgate,
    w_cgate,
    w_attn_out,
    w_conv_out,
    sink_logit,
    taps,
    conv_bias,
    documents,
):
    f32 = jnp.float32
    bf16 = jnp.bfloat16
    rows, part = tokens.shape
    tp_count = lax.axis_size("tp")
    sp_count = lax.axis_size("sp")
    width = part * tp_count
    head_dim = HEAD_DIM
    q_local = w_query.shape[1] // head_dim
    kv_local = w_key.shape[1] // head_dim
    groups = q_local // kv_local
    wq, wk, wv, wu, wb, wc, w_attn, w_conv = (
        lax.all_gather(w_query, "sp", axis=0, tiled=True),
        lax.all_gather(w_key, "sp", axis=0, tiled=True),
        lax.all_gather(w_value, "sp", axis=0, tiled=True),
        lax.all_gather(w_input, "sp", axis=0, tiled=True),
        lax.all_gather(w_bgate, "sp", axis=0, tiled=True),
        lax.all_gather(w_cgate, "sp", axis=0, tiled=True),
        lax.all_gather(w_attn_out, "sp", axis=0, tiled=True),
        lax.all_gather(w_conv_out, "sp", axis=0, tiled=True),
    )
    matrices = (wq, wk, wv, wu, wb, wc)
    piece_f = lax.all_gather(tokens, "tp", axis=1, tiled=True).astype(f32)
    scaled = (piece_f * gain[None, :]).astype(bf16)
    products = tuple((jnp.dot(scaled, mat, preferred_element_type=f32) for mat in matrices))
    folded = products + (jnp.sum(piece_f * piece_f, axis=1),)
    sums = folded[:6]
    squares = folded[6]
    inv = lax.rsqrt(squares / width + EPS)[:, None]
    q_acc, k_acc, v_acc, u_acc, b_acc, c_acc = sums
    positions = lax.axis_index("sp") * rows + jnp.arange(rows, dtype=jnp.int32)
    query = rotate(q_acc * inv, positions, q_local).astype(bf16)
    keys = rotate(k_acc * inv, positions, kv_local).astype(bf16)
    values = (v_acc * inv).astype(bf16)
    carried = (c_acc * inv * (u_acc * inv)).astype(bf16)
    bgate = b_acc * inv
    doc_col = documents.astype(f32).astype(bf16)[:, None]
    paired = jnp.concatenate([keys, values], axis=1)
    pair_ext, doc_ext = (
        extended(paired, (("sp", 0),), WINDOW),
        extended(doc_col, (("sp", 0),), WINDOW),
    )
    carry_ext, doc_near = (extended(carried, (("sp", 0),), 1), extended(doc_col, (("sp", 0),), 1))
    key_width = kv_local * head_dim
    key_ext = pair_ext[:, :key_width].reshape(-1, kv_local, head_dim)
    val_ext = pair_ext[:, key_width:].reshape(-1, kv_local, head_dim)
    key_doc = doc_ext[:, 0].astype(f32)
    own_doc = doc_col[:, 0].astype(f32)
    key_pos = positions[0] - WINDOW + jnp.arange(rows + 2 * WINDOW, dtype=jnp.int32)
    total = sp_count * rows
    sinks = sink_logit.reshape(kv_local, groups, 1, 1)
    block = rows // 2
    outputs = []
    for begin in range(0, rows, block):
        span = block + 2 * WINDOW
        q_block = query[begin : begin + block].reshape(block, kv_local, groups, head_dim)
        k_block = key_ext[begin : begin + span]
        v_block = val_ext[begin : begin + span]
        q_pos = positions[begin : begin + block]
        k_pos = key_pos[begin : begin + span]
        scores = jnp.einsum(
            "qhgd,khd->hgqk", q_block, k_block, preferred_element_type=f32
        ) * head_dim ** (-0.5)
        allowed = jnp.abs(q_pos[:, None] - k_pos[None, :]) <= WINDOW
        allowed = allowed & (
            own_doc[begin : begin + block, None] == key_doc[None, begin : begin + span]
        )
        allowed = allowed & (k_pos >= 0)[None, :] & (k_pos < total)[None, :]
        weight = sink_softmax(scores, allowed, sinks).astype(bf16)
        result = jnp.einsum("hgqk,khd->qhgd", weight, v_block, preferred_element_type=f32)
        outputs.append(result.astype(bf16).reshape(block, q_local * head_dim))
    attended = jnp.concatenate(outputs, axis=0)
    near_doc = doc_near[:, 0].astype(f32)
    conv = jnp.zeros((rows, carried.shape[1]), f32)
    for tap in range(3):
        same = (near_doc[tap : tap + rows] == near_doc[1 : rows + 1])[:, None]
        conv = conv + jnp.where(
            same, carry_ext[tap : tap + rows].astype(f32) * taps[tap][None, :], 0.0
        )
    convolved = (bgate * (conv + conv_bias[None, :])).astype(bf16)
    acc = jnp.dot(
        lax.all_gather(attended, "tp", axis=1, tiled=True), w_attn, preferred_element_type=f32
    )
    mixed = acc + jnp.dot(
        lax.all_gather(convolved, "tp", axis=1, tiled=True), w_conv, preferred_element_type=f32
    )
    return mixed.astype(bf16)


def solution(mesh):
    placed = (
        P(("grp", "sp"), "tp"),
        P(),
        P("sp", "tp"),
        P("sp", "tp"),
        P("sp", "tp"),
        P("sp", "tp"),
        P("sp", "tp"),
        P("sp", "tp"),
        P("sp", "tp"),
        P("sp", "tp"),
        P("tp"),
        P(None, "tp"),
        P("tp"),
        P(("grp", "sp")),
    )
    return jax.shard_map(
        local, mesh=mesh, in_specs=placed, out_specs=P(("grp", "sp"), "tp"), check_vma=False
    )
```

profile of v0, /device:TPU:0, one launch (start us, length us, event | category | flops | bytes accessed | tf_op | source)
XLA Modules:
  0.0 308.4 jit_solution(10480472641820720276)
XLA Ops:
  12.0 3.0 collective-permute-start.1
  16.3 17.1 %all_gather.35 = bf16[2048,128]{1,0:T(8,128)(2,1)S(1)} all-gather(bf16[256,128]{1,0:T(8,128)(2,1)} %param.18), channel_id=1, replica_groups=mesh['grp'=2,'sp'=8,'tp'=2] {'sp'}, dimensions={0}, use_global_device_ids=true | all-gather | bytes 589824 | tf_op jit(solution)/shard_map/all_gather | solution.py:82
  33.4 14.7 %all_gather.34 = bf16[2048,128]{1,0:T(8,128)(2,1)S(1)} all-gather(bf16[256,128]{1,0:T(8,128)(2,1)S(1)} %copy-done.3), channel_id=1, replica_groups=mesh['grp'=2,'sp'=8,'tp'=2] {'sp'}, dimensions={0}, use_global_device_ids=true | all-gather | bytes 589824 | tf_op jit(solution)/shard_map/all_gather | solution.py:81
  49.4 7.1 %all-gather.10.cloned.1.call-done = bf16[768,2048]{1,0:T(8,128)(2,1)} async-done(((bf16[768,1024]{1,0:T(8,128)(2,1)}), bf16[768,2048]{1,0:T(8,128)(2,1)}) %all-gather.10.cloned.1.call-update) | async-done | bytes 3145744 | tf_op jit(solution)/shard_map/all_gather | solution.py:90
  56.5 2.7 fusion.3
  65.7 2.3 collective-permute-done.3
  68.1 19.9 %all-gather.12.cloned.1.call-done = bf16[2048,512]{1,0:T(8,128)(2,1)} async-done(((bf16[256,512]{1,0:T(8,128)(2,1)}), bf16[2048,512]{1,0:T(8,128)(2,1)}) %all-gather.12.cloned.1.call-update) | async-done | bytes 2097168 | tf_op jit(solution)/shard_map/all_gather | solution.py:80
  88.0 4.4 %convolution_multiply_fusion = f32[768,512]{0,1:T(8,128)S(1)} fusion(bf16[2048,512]{1,0:T(8,128)(2,1)} %all-gather.12.cloned.1.call-done, bf16[768,2048]{1,0:T(8,128)(2,1)} %all-gather.10.cloned.1.call-done, f32[2048]{0:T(1024)S(1)} %copy-done.5, f32[768]{0:T(1024)S(1)} %add_rsqrt_fusion), kind=kOutput, calls=%fused_computation.19 | convolution fusion | flops 1615724544 | bytes 6827008 | tf_op jit(solution)/shard_map/dot_general | solution.py:92
  99.0 2.6 fusion.18
  101.6 2.6 fusion.19
  107.8 3.6 %collective-permute-start.4 = (bf16[1,1]{0,1:T(2,128)(2,1)}, bf16[1,1]{0,1:T(2,128)(2,1)}, u32[]{:S(2)}, u32[]{:S(2)}) collective-permute-start(bf16[1,1]{0,1:T(2,128)(2,1)} %bitcast.26), channel_id=1, source_target_pairs={{0,2},{2,4},{4,6},{6,8},{8,10},{10,12},{12,14},{1,3},{3,5},{5,7},{... | collective-permute-start | bytes 14 | tf_op jit(solution)/shard_map/ppermute | solution.py:20
  113.2 5.0 %all-gather.20.cloned.1.call-done = bf16[2048,512]{1,0:T(8,128)(2,1)} async-done(((bf16[256,512]{1,0:T(8,128)(2,1)}), bf16[2048,512]{1,0:T(8,128)(2,1)}) %all-gather.20.cloned.1.call-update) | async-done | bytes 2097168 | tf_op jit(solution)/shard_map/all_gather | solution.py:85
  118.2 5.5 %fusion.9 = f32[768,512]{0,1:T(8,128)} fusion(bf16[2048,512]{1,0:T(8,128)(2,1)} %all-gather.20.cloned.1.call-done, bf16[768,2048]{1,0:T(8,128)(2,1)} %all-gather.10.cloned.1.call-done, f32[2048]{0:T(1024)S(1)} %copy-done.5), kind=kOutput, calls=%fused_computation.20 | convolution fusion | flops 1615331328 | bytes 6823936 | tf_op jit(solution)/shard_map/dot_general | solution.py:92
  123.7 24.5 %all-gather.22.cloned.1.call-done = bf16[2048,512]{1,0:T(8,128)(2,1)} async-done(((bf16[256,512]{1,0:T(8,128)(2,1)}), bf16[2048,512]{1,0:T(8,128)(2,1)}) %all-gather.22.cloned.1.call-update) | async-done | bytes 2097168 | tf_op jit(solution)/shard_map/all_gather | solution.py:83
  148.2 3.9 %multiply_convert_fusion.1 = bf16[768,512]{0,1:T(8,128)(2,1)S(1)} fusion(f32[768,512]{0,1:T(8,128)} %fusion.9, bf16[2048,512]{1,0:T(8,128)(2,1)} %all-gather.22.cloned.1.call-done, bf16[768,2048]{1,0:T(8,128)(2,1)S(1)} %copy-done.1, f32[2048]{0:T(1024)S(1)} %copy-done.5, f32[768]{0:T(1024)S(1)} %add_rsqrt_fusion), kind=kOutput, calls=%fused_computation.18 | convolution fusion | flops 1616904192 | bytes 7613440 | tf_op jit(solution)/shard_map/dot_general | solution.py:92
  153.6 3.7 %collective-permute-start.6 = (bf16[1,512]{0,1:T(8,128)(2,1)S(1)}, bf16[1,512]{0,1:T(8,128)(2,1)}, u32[]{:S(2)}, u32[]{:S(2)}) collective-permute-start(bf16[1,512]{0,1:T(8,128)(2,1)S(1)} %get-tuple-element.12), channel_id=1, source_target_pairs={{0,2},{2,4},{4,6},{6,8},{8,10},{10,12},{12,14},{1,3},{3,5},{5,7},{... | collective-permute-start | bytes 3080 | tf_op jit(solution)/shard_map/ppermute | solution.py:20
  157.4 20.9 %all-gather.18.cloned.1.call-done = bf16[2048,512]{1,0:T(8,128)(2,1)} async-done(((bf16[256,512]{1,0:T(8,128)(2,1)}), bf16[2048,512]{1,0:T(8,128)(2,1)}) %all-gather.18.cloned.1.call-update) | async-done | bytes 2097168 | tf_op jit(solution)/shard_map/all_gather | solution.py:84
  178.3 5.7 %multiply_convert_fusion = bf16[768,512]{0,1:T(8,128)(2,1)} fusion(bf16[768,512]{0,1:T(8,128)(2,1)} %copy-done.2, bf16[1,512]{0,1:T(8,128)(2,1)} %collective-permute-done.7, bf16[1,512]{0,1:T(8,128)(2,1)} %collective-permute-done.6, f32[512]{0:T(512)S(1)} %copy-done.6, f32[512]{0:T(512)S(1)} %bitcast.92, f32[512]{0:T(512)S(1)} %bitcast.93, ...), kind=kOutput, calls=%fused_computation.17 | convolution fusion | flops 1623588864 | bytes 6839552 | tf_op jit(solution)/shard_map/dot_general | solution.py:92
  184.0 25.7 %all-gather.16.cloned.1.call-done = bf16[1024,1024]{1,0:T(8,128)(2,1)} async-done(((bf16[128,1024]{1,0:T(8,128)(2,1)}), bf16[1024,1024]{1,0:T(8,128)(2,1)}) %all-gather.16.cloned.1.call-update) | async-done | bytes 2097168 | tf_op jit(solution)/shard_map/all_gather | solution.py:86
  209.7 28.1 %all-gather.14.cloned.1.call-done = bf16[768,1024]{0,1:T(8,128)(2,1)} async-done(((bf16[768,512]{0,1:T(8,128)(2,1)}), bf16[768,1024]{0,1:T(8,128)(2,1)}) %all-gather.14.cloned.1.call-update) | async-done | bytes 1572880 | tf_op jit(solution)/shard_map/all_gather | solution.py:149
  237.8 3.9 %fusion.47 = f32[768,1024]{1,0:T(8,128)S(1)} fusion(bf16[768,1024]{0,1:T(8,128)(2,1)} %all-gather.14.cloned.1.call-done, bf16[1024,1024]{1,0:T(8,128)(2,1)} %all-gather.16.cloned.1.call-done), kind=kOutput, calls=%fused_computation.92 | convolution fusion | flops 1610612736 | bytes 6815744 | tf_op jit(solution)/shard_map/dot_general | solution.py:148
  241.7 26.9 %all-gather.26.cloned.1.call-done = bf16[1024,1024]{1,0:T(8,128)(2,1)} async-done(((bf16[128,1024]{1,0:T(8,128)(2,1)}), bf16[1024,1024]{1,0:T(8,128)(2,1)}) %all-gather.26.cloned.1.call-update) | async-done | bytes 2097168 | tf_op jit(solution)/shard_map/all_gather | solution.py:87
  268.6 28.2 %all-gather.24.cloned.1.call-done = bf16[768,1024]{0,1:T(8,128)(2,1)} async-done(((bf16[768,512]{0,1:T(8,128)(2,1)}), bf16[768,1024]{0,1:T(8,128)(2,1)}) %all-gather.24.cloned.1.call-update) | async-done | bytes 1572880 | tf_op jit(solution)/shard_map/all_gather | solution.py:152
  296.8 5.0 %add_convert_fusion = bf16[768,1024]{1,0:T(8,128)(2,1)} fusion(f32[768,1024]{1,0:T(8,128)S(1)} %fusion.47, bf16[768,1024]{0,1:T(8,128)(2,1)} %all-gather.24.cloned.1.call-done, bf16[1024,1024]{1,0:T(8,128)(2,1)} %all-gather.26.cloned.1.call-done), kind=kOutput, calls=%fused_computation.16 | convolution fusion | flops 1612185600 | bytes 8388608 | tf_op jit(solution)/shard_map/dot_general | solution.py:151
  (85 shorter events, 27.2 us)
Async XLA Ops:
  6.5 26.9 %copy-start.3 = (bf16[256,128]{1,0:T(8,128)(2,1)S(1)}, bf16[256,128]{1,0:T(8,128)(2,1)}, u32[]{:S(2)}) copy-start(bf16[256,128]{1,0:T(8,128)(2,1)} %param.17) | copy-start | bytes 196612
  6.5 42.0 %copy-start.7 = (f32[8]{0:T(128)S(1)}, f32[8]{0:T(128)}, u32[]{:S(2)}) copy-start(f32[8]{0:T(128)} %param.24) | copy-start | bytes 100
  6.5 50.0 %all-gather.10.cloned.1.call-start = ((), (), s32[]{:S(2)}) async-start(), calls=%async_computation | async-start | bytes 4718592 | tf_op jit(solution)/shard_map/all_gather | solution.py:90
  7.3 52.0 %copy-start.5 = (f32[2048]{0:T(1024)S(1)}, f32[2048]{0:T(1024)}, u32[]{:S(2)}) copy-start(f32[2048]{0:T(1024)} %param.15) | copy-start | bytes 24580
  7.3 80.8 %all-gather.12.cloned.1.call-start = ((), (), s32[]{:S(2)}) async-start(), calls=%async_computation.1 | async-start | bytes 2359296 | tf_op jit(solution)/shard_map/all_gather | solution.py:80
  8.0 110.2 %all-gather.20.cloned.1.call-start = ((), (), s32[]{:S(2)}) async-start(), calls=%async_computation.5 | async-start | bytes 2359296 | tf_op jit(solution)/shard_map/all_gather | solution.py:85
  8.8 139.5 %all-gather.22.cloned.1.call-start = ((), (), s32[]{:S(2)}) async-start(), calls=%async_computation.6 | async-start | bytes 2359296 | tf_op jit(solution)/shard_map/all_gather | solution.py:83
  9.3 168.9 %all-gather.18.cloned.1.call-start = ((), (), s32[]{:S(2)}) async-start(), calls=%async_computation.4 | async-start | bytes 2359296 | tf_op jit(solution)/shard_map/all_gather | solution.py:84
  9.9 199.8 %all-gather.16.cloned.1.call-start = ((), (), s32[]{:S(2)}) async-start(), calls=%async_computation.3 | async-start | bytes 2359296 | tf_op jit(solution)/shard_map/all_gather | solution.py:86
  10.7 38.0 %collective-permute-start.2 = (bf16[128,1]{0,1:T(2,128)(2,1)S(1)}, bf16[128,1]{0,1:T(2,128)(2,1)S(1)}, u32[]{:S(2)}, u32[]{:S(2)}) collective-permute-start(bf16[128,1]{0,1:T(2,128)(2,1)S(1)} %get-tuple-element.44), channel_id=1, source_target_pairs={{2,0},{4,2},{6,4},{8,6},{10,8},{12,10},{14,12},{3,1},{5,3},{7,5},{... | collective-permute-start | bytes 776 | tf_op jit(solution)/shard_map/ppermute | solution.py:22
  12.0 36.7 %collective-permute-start.1 = (bf16[128,1]{0,1:T(2,128)(2,1)S(1)}, bf16[128,1]{0,1:T(2,128)(2,1)S(1)}, u32[]{:S(2)}, u32[]{:S(2)}) collective-permute-start(bf16[128,1]{0,1:T(2,128)(2,1)S(1)} %get-tuple-element.43), channel_id=1, source_target_pairs={{0,2},{2,4},{4,6},{6,8},{8,10},{10,12},{12,14},{1,3},{3,5},{5,7},{... | collective-permute-start | bytes 776 | tf_op jit(solution)/shard_map/ppermute | solution.py:20
  15.0 222.8 %all-gather.14.cloned.1.call-start = ((), (), s32[]{:S(2)}) async-start(), calls=%async_computation.2 | async-start | bytes 2359296 | tf_op jit(solution)/shard_map/all_gather | solution.py:149
  61.9 3.8 %collective-permute-start = (bf16[128,256]{0,1:T(8,128)(2,1)S(1)}, bf16[128,256]{0,1:T(8,128)(2,1)S(1)}, u32[]{:S(2)}, u32[]{:S(2)}) collective-permute-start(bf16[128,256]{0,1:T(8,128)(2,1)S(1)} %get-tuple-element.24), channel_id=1, source_target_pairs={{0,2},{2,4},{4,6},{6,8},{8,10},{10,12},{12,14},{1,3},{3,5},{5,7},{... | collective-permute-start | bytes 196616 | tf_op jit(solution)/shard_map/ppermute | solution.py:20
  63.5 4.6 %collective-permute-start.3 = (bf16[128,256]{0,1:T(8,128)(2,1)S(1)}, bf16[128,256]{0,1:T(8,128)(2,1)S(1)}, u32[]{:S(2)}, u32[]{:S(2)}) collective-permute-start(bf16[128,256]{0,1:T(8,128)(2,1)S(1)} %get-tuple-element.25), channel_id=1, source_target_pairs={{2,0},{4,2},{6,4},{8,6},{10,8},{12,10},{14,12},{3,1},{5,3},{7,5},{... | collective-permute-start | bytes 196616 | tf_op jit(solution)/shard_map/ppermute | solution.py:22
  101.6 9.9 %copy-start.4 = (f32[3,512]{1,0:T(4,128)S(1)}, f32[3,512]{1,0:T(4,128)}, u32[]{:S(2)}) copy-start(f32[3,512]{1,0:T(4,128)} %param.25) | copy-start | bytes 18436
  105.1 163.5 %all-gather.26.cloned.1.call-start = ((), (), s32[]{:S(2)}) async-start(), calls=%async_computation.8 | async-start | bytes 2359296 | tf_op jit(solution)/shard_map/all_gather | solution.py:87
  105.9 190.9 %all-gather.24.cloned.1.call-start = ((), (), s32[]{:S(2)}) async-start(), calls=%async_computation.7 | async-start | bytes 2359296 | tf_op jit(solution)/shard_map/all_gather | solution.py:152
  106.5 4.9 %collective-permute-start.5 = (bf16[1,1]{0,1:T(2,128)(2,1)}, bf16[1,1]{0,1:T(2,128)(2,1)}, u32[]{:S(2)}, u32[]{:S(2)}) collective-permute-start(bf16[1,1]{0,1:T(2,128)(2,1)} %bitcast.27), channel_id=1, source_target_pairs={{2,0},{4,2},{6,4},{8,6},{10,8},{12,10},{14,12},{3,1},{5,3},{7,5},{... | collective-permute-start | bytes 14 | tf_op jit(solution)/shard_map/ppermute | solution.py:22
  107.8 4.0 %collective-permute-start.4 = (bf16[1,1]{0,1:T(2,128)(2,1)}, bf16[1,1]{0,1:T(2,128)(2,1)}, u32[]{:S(2)}, u32[]{:S(2)}) collective-permute-start(bf16[1,1]{0,1:T(2,128)(2,1)} %bitcast.26), channel_id=1, source_target_pairs={{0,2},{2,4},{4,6},{6,8},{8,10},{10,12},{12,14},{1,3},{3,5},{5,7},{... | collective-permute-start | bytes 14 | tf_op jit(solution)/shard_map/ppermute | solution.py:20
  113.2 35.0 %copy-start.1 = (bf16[768,2048]{1,0:T(8,128)(2,1)S(1)}, bf16[768,2048]{1,0:T(8,128)(2,1)}, u32[]{:S(2)}) copy-start(bf16[768,2048]{1,0:T(8,128)(2,1)} %all-gather.10.cloned.1.call-done) | copy-start | bytes 9437188
  123.7 54.5 %copy-start.6 = (f32[512]{0:T(512)S(1)}, f32[512]{0:T(512)}, u32[]{:S(2)}) copy-start(f32[512]{0:T(512)} %param.26) | copy-start | bytes 6148
  152.1 5.1 %copy-start.2 = (bf16[768,512]{0,1:T(8,128)(2,1)}, bf16[768,512]{0,1:T(8,128)(2,1)S(1)}, u32[]{:S(2)}) copy-start(bf16[768,512]{0,1:T(8,128)(2,1)S(1)} %multiply_convert_fusion.1) | copy-start | bytes 2359300
  152.3 26.0 %collective-permute-start.7 = (bf16[1,512]{0,1:T(8,128)(2,1)S(1)}, bf16[1,512]{0,1:T(8,128)(2,1)}, u32[]{:S(2)}, u32[]{:S(2)}) collective-permute-start(bf16[1,512]{0,1:T(8,128)(2,1)S(1)} %get-tuple-element.13), channel_id=1, source_target_pairs={{2,0},{4,2},{6,4},{8,6},{10,8},{12,10},{14,12},{3,1},{5,3},{7,5},{... | collective-permute-start | bytes 3080 | tf_op jit(solution)/shard_map/ppermute | solution.py:22
  153.6 24.7 %collective-permute-start.6 = (bf16[1,512]{0,1:T(8,128)(2,1)S(1)}, bf16[1,512]{0,1:T(8,128)(2,1)}, u32[]{:S(2)}, u32[]{:S(2)}) collective-permute-start(bf16[1,512]{0,1:T(8,128)(2,1)S(1)} %get-tuple-element.12), channel_id=1, source_target_pairs={{0,2},{2,4},{4,6},{6,8},{8,10},{10,12},{12,14},{1,3},{3,5},{5,7},{... | collective-permute-start | bytes 3080 | tf_op jit(solution)/shard_map/ppermute | solution.py:20
  (1 other events, 2.8 us)
Sparse Core Ops, SparseCore 0:
  8.9 47.6 all-gather.9
  58.1 29.8 all-gather.11
  89.6 28.5 all-gather.19
  119.7 28.5 all-gather.21
  149.7 28.5 all-gather.17
  179.7 29.9 all-gather.15
  211.2 26.5 all-gather.13
  239.4 29.1 all-gather.25
  270.2 26.5 all-gather.23
where the time goes:
time: 309 us; the launch traced here: 308 us
  waiting for transfers between devices  193 us (62%)
  matrix products  38.7 us (13%)
  blocking collectives  31.8 us (10%)
  starting transfers between devices  17.6 us (6%)
  between operations  14.2 us (5%)
  other arithmetic  11.9 us (4%)
    all_gather x1, waiting for transfers between devices, local(): lax.all_gather(convolved, 'tp', axis=1, tiled=True)  28.2 us
    all_gather x1, waiting for transfers between devices, local(): lax.all_gather(attended, 'tp', axis=1, tiled=True)  28.1 us
    all_gather x1, waiting for transfers between devices, local(): lax.all_gather(w_conv_out, 'sp', axis=0, tiled=True)  26.9 us
    all_gather x1, waiting for transfers between devices, local(): lax.all_gather(w_attn_out, 'sp', axis=0, tiled=True)  25.7 us
    all_gather x1, waiting for transfers between devices, local(): lax.all_gather(w_input, 'sp', axis=0, tiled=True)  24.5 us
    dot_general x6, matrix products, local(): jnp.dot(scaled, mat, preferred_element_type=f32)  21.9 us
    all_gather x1, waiting for transfers between devices, local(): lax.all_gather(w_bgate, 'sp', axis=0, tiled=True)  20.9 us
    all_gather x1, waiting for transfers between devices, local(): lax.all_gather(w_query, 'sp', axis=0, tiled=True)  19.9 us
  transfers between devices with their start and end apart: 17, of which 11 were waited for; matrix products, arithmetic and copies ran while one was open for 15% of the time, Pallas kernels for 0%

commit v1 on v0

--- a/solution.py
+++ b/solution.py
@@ -80,7 +80,9 @@
         lax.all_gather(w_query, "sp", axis=0, tiled=True),
         lax.all_gather(w_key, "sp", axis=0, tiled=True),
         lax.all_gather(w_value, "sp", axis=0, tiled=True),
-        lax.all_gather(w_input, "sp", axis=0, tiled=True),
+        jnp.concatenate(
+            lax.all_to_all(jnp.stack([w_input] * lax.axis_size("sp")), "sp", 0, 0), axis=0
+        ),
         lax.all_gather(w_bgate, "sp", axis=0, tiled=True),
         lax.all_gather(w_cgate, "sp", axis=0, tiled=True),
         lax.all_gather(w_attn_out, "sp", axis=0, tiled=True),

time: 309 us -> 287 us (0.929)
  waiting for transfers between devices: 193 us -> 102 us
  blocking collectives: 31.8 us -> 87.5 us
  starting transfers between devices: 17.6 us -> 28.1 us
    all_gather x1, blocking collectives: 17.1 us -> 69.9 us  [local(): lax.all_gather(w_value, 'sp', axis=0, tiled=True)]
    all_gather x1 -> x0, waiting for transfers between devices: 24.5 us -> none  [local(): lax.all_gather(w_input, 'sp', axis=0, tiled=True)]
    all_gather x1, waiting for transfers between devices: 20.9 us -> 0.02 us  [local(): lax.all_gather(w_bgate, 'sp', axis=0, tiled=True)]
    all_gather x1, waiting for transfers between devices: 19.9 us -> 0.02 us  [local(): lax.all_gather(w_query, 'sp', axis=0, tiled=True)]
    all_gather x1, waiting for transfers between devices: 25.7 us -> 12.2 us  [local(): lax.all_gather(w_attn_out, 'sp', axis=0, tiled=True)]
    all_gather x1, waiting for transfers between devices: 7.12 us -> 0.02 us  [local(): piece_f = lax.all_gather(tokens, 'tp', axis=1, tiled=True).astype(f32)]
    all_to_all x0 -> x1, starting transfers between devices: none -> 6.49 us  [local(): lax.all_to_all(jnp.stack([w_input] * lax.axis_size('sp')), 'sp', 0, 0)]
    all_gather x1, waiting for transfers between devices: 4.96 us -> 0.01 us  [local(): lax.all_gather(w_cgate, 'sp', axis=0, tiled=True)]
  transfers between devices with their start and end apart: 17 -> 17, of which waited for: 11 -> 7; matrix products, arithmetic and copies ran while one was open for 15% -> 17% of each run, Pallas kernels for 0% -> 0%
where the time goes in v1:
time: 287 us; the launch traced here: 286 us
  waiting for transfers between devices  102 us (36%)
  blocking collectives  87.5 us (30%)
  matrix products  38.8 us (14%)
  starting transfers between devices  28.1 us (10%)
  between operations  14.5 us (5%)
  other arithmetic  11.7 us (4%)
  local copies, waits for them, and re-layouts  3.97 us (1%)
    all_gather x1, blocking collectives, local(): lax.all_gather(w_value, 'sp', axis=0, tiled=True)  69.9 us
    all_gather x1, waiting for transfers between devices, local(): lax.all_gather(convolved, 'tp', axis=1, tiled=True)  28.1 us
    all_gather x1, waiting for transfers between devices, local(): lax.all_gather(attended, 'tp', axis=1, tiled=True)  28 us
    all_gather x1, waiting for transfers between devices, local(): lax.all_gather(w_conv_out, 'sp', axis=0, tiled=True)  26.9 us
    dot_general x6, matrix products, local(): jnp.dot(scaled, mat, preferred_element_type=f32)  22.1 us
    all_gather x1, blocking collectives, local(): lax.all_gather(w_key, 'sp', axis=0, tiled=True)  17.6 us
    ppermute x4, starting transfers between devices, extended(): lax.ppermute(tail, axis, [(i, (i + 1) % count) for i in range(ends)])  16 us
    all_gather x1, waiting for transfers between devices, local(): lax.all_gather(w_attn_out, 'sp', axis=0, tiled=True)  12.2 us
  transfers between devices with their start and end apart: 17, of which 7 were waited for; matrix products, arithmetic and copies ran while one was open for 17% of the time, Pallas kernels for 0%

profile of v1, /device:TPU:0, one launch (start us, length us, event | category | flops | bytes accessed | tf_op | source)
XLA Modules:
  0.0 286.5 jit_solution(15820729081790867719)
XLA Ops:
  11.3 3.2 %collective-permute-start.1 = (bf16[128,1]{0,1:T(2,128)(2,1)S(1)}, bf16[128,1]{0,1:T(2,128)(2,1)S(1)}, u32[]{:S(2)}, u32[]{:S(2)}) collective-permute-start(bf16[128,1]{0,1:T(2,128)(2,1)S(1)} %get-tuple-element.43), channel_id=1, source_target_pairs={{0,2},{2,4},{4,6},{6,8},{8,10},{10,12},{12,14},{1,3},{3,5},{5,7},{... | collective-permute-start | bytes 776 | tf_op jit(solution)/shard_map/ppermute | solution.py:20
  14.5 2.5 stack.2
  16.9 6.5 %all-to-all-start = ((bf16[8,256,512]{2,1,0:T(8,128)(2,1)}), bf16[8,256,512]{2,1,0:T(8,128)(2,1)}, u32[]{:S(2)}, u32[]{:S(2)}) async-start(bf16[8,256,512]{2,1,0:T(8,128)(2,1)} %stack.2), calls=%async_computation | async-start | bytes 4194304 | tf_op jit(solution)/shard_map/all_to_all | solution.py:84
  25.3 69.9 %all_gather.32 = bf16[2048,128]{1,0:T(8,128)(2,1)S(1)} all-gather(bf16[256,128]{1,0:T(8,128)(2,1)S(1)} %copy-done.3), channel_id=1, replica_groups=mesh['grp'=2,'sp'=8,'tp'=2] {'sp'}, dimensions={0}, use_global_device_ids=true | all-gather | bytes 589824 | tf_op jit(solution)/shard_map/all_gather | solution.py:82
  95.3 17.6 %all_gather.31 = bf16[2048,128]{1,0:T(8,128)(2,1)S(1)} all-gather(bf16[256,128]{1,0:T(8,128)(2,1)S(1)} %copy-done.4), channel_id=1, replica_groups=mesh['grp'=2,'sp'=8,'tp'=2] {'sp'}, dimensions={0}, use_global_device_ids=true | all-gather | bytes 589824 | tf_op jit(solution)/shard_map/all_gather | solution.py:81
  114.2 2.7 fusion.3
  119.6 2.3 collective-permute-start
  124.1 1.7 collective-permute-done.3
  125.9 4.4 %convolution_multiply_fusion = f32[768,512]{0,1:T(8,128)S(1)} fusion(bf16[2048,512]{1,0:T(8,128)(2,1)} %all-gather.11.cloned.1.call-done, bf16[768,2048]{1,0:T(8,128)(2,1)} %all-gather.9.cloned.1.call-done, f32[2048]{0:T(1024)S(1)} %copy-done.6, f32[768]{0:T(1024)S(1)} %add_rsqrt_fusion), kind=kOutput, calls=%fused_computation.19 | convolution fusion | flops 1615724544 | bytes 6827008 | tf_op jit(solution)/shard_map/dot_general | solution.py:94
  132.1 1.6 fusion
  135.2 1.7 fusion.1
  136.9 2.6 fusion.18
  139.5 2.6 fusion.19
  145.7 6.0 %collective-permute-start.4 = (bf16[1,1]{0,1:T(2,128)(2,1)}, bf16[1,1]{0,1:T(2,128)(2,1)}, u32[]{:S(2)}, u32[]{:S(2)}) collective-permute-start(bf16[1,1]{0,1:T(2,128)(2,1)} %bitcast.26), channel_id=1, source_target_pairs={{0,2},{2,4},{4,6},{6,8},{8,10},{10,12},{12,14},{1,3},{3,5},{5,7},{... | collective-permute-start | bytes 14 | tf_op jit(solution)/shard_map/ppermute | solution.py:20
  153.6 5.7 %fusion.9 = f32[768,512]{0,1:T(8,128)} fusion(bf16[2048,512]{1,0:T(8,128)(2,1)} %all-gather.19.cloned.1.call-done, bf16[768,2048]{1,0:T(8,128)(2,1)} %all-gather.9.cloned.1.call-done, f32[2048]{0:T(1024)S(1)} %copy-done.6), kind=kOutput, calls=%fused_computation.20 | convolution fusion | flops 1615331328 | bytes 6823936 | tf_op jit(solution)/shard_map/dot_general | solution.py:94
  159.3 3.9 %multiply_convert_fusion.1 = bf16[768,512]{0,1:T(8,128)(2,1)S(1)} fusion(f32[768,512]{0,1:T(8,128)} %fusion.9, bf16[2048,512]{1,0:T(8,128)(2,1)} %bitcast.28, bf16[768,2048]{1,0:T(8,128)(2,1)S(1)} %copy-done.1, f32[2048]{0:T(1024)S(1)} %copy-done.6, f32[768]{0:T(1024)S(1)} %add_rsqrt_fusion), kind=kOutput, calls=%fused_computation.18 | convolution fusion | flops 1616904192 | bytes 7613440 | tf_op jit(solution)/shard_map/dot_general | solution.py:94
  164.6 4.7 %collective-permute-start.6 = (bf16[1,512]{0,1:T(8,128)(2,1)S(1)}, bf16[1,512]{0,1:T(8,128)(2,1)}, u32[]{:S(2)}, u32[]{:S(2)}) collective-permute-start(bf16[1,512]{0,1:T(8,128)(2,1)S(1)} %get-tuple-element.12), channel_id=1, source_target_pairs={{0,2},{2,4},{4,6},{6,8},{8,10},{10,12},{12,14},{1,3},{3,5},{5,7},{... | collective-permute-start | bytes 3080 | tf_op jit(solution)/shard_map/ppermute | solution.py:20
  169.8 5.7 %multiply_convert_fusion = bf16[768,512]{0,1:T(8,128)(2,1)} fusion(bf16[768,512]{0,1:T(8,128)(2,1)} %copy-done.2, bf16[1,512]{0,1:T(8,128)(2,1)} %collective-permute-done.7, bf16[1,512]{0,1:T(8,128)(2,1)} %collective-permute-done.6, f32[512]{0:T(512)S(1)} %copy-done.7, f32[512]{0:T(512)S(1)} %bitcast.93, f32[512]{0:T(512)S(1)} %bitcast.94, ...), kind=kOutput, calls=%fused_computation.17 | convolution fusion | flops 1623588864 | bytes 6839552 | tf_op jit(solution)/shard_map/dot_general | solution.py:94
  175.5 12.2 %all-gather.15.cloned.1.call-done = bf16[1024,1024]{1,0:T(8,128)(2,1)} async-done(((bf16[128,1024]{1,0:T(8,128)(2,1)}), bf16[1024,1024]{1,0:T(8,128)(2,1)}) %all-gather.15.cloned.1.call-update) | async-done | bytes 2097168 | tf_op jit(solution)/shard_map/all_gather | solution.py:88
  187.6 28.0 %all-gather.13.cloned.1.call-done = bf16[768,1024]{0,1:T(8,128)(2,1)} async-done(((bf16[768,512]{0,1:T(8,128)(2,1)}), bf16[768,1024]{0,1:T(8,128)(2,1)}) %all-gather.13.cloned.1.call-update) | async-done | bytes 1572880 | tf_op jit(solution)/shard_map/all_gather | solution.py:151
  215.6 3.9 %fusion.47 = f32[768,1024]{1,0:T(8,128)S(1)} fusion(bf16[768,1024]{0,1:T(8,128)(2,1)} %all-gather.13.cloned.1.call-done, bf16[1024,1024]{1,0:T(8,128)(2,1)} %all-gather.15.cloned.1.call-done), kind=kOutput, calls=%fused_computation.92 | convolution fusion | flops 1610612736 | bytes 6815744 | tf_op jit(solution)/shard_map/dot_general | solution.py:150
  219.5 26.9 %all-gather.23.cloned.1.call-done = bf16[1024,1024]{1,0:T(8,128)(2,1)} async-done(((bf16[128,1024]{1,0:T(8,128)(2,1)}), bf16[1024,1024]{1,0:T(8,128)(2,1)}) %all-gather.23.cloned.1.call-update) | async-done | bytes 2097168 | tf_op jit(solution)/shard_map/all_gather | solution.py:89
  246.4 28.1 %all-gather.21.cloned.1.call-done = bf16[768,1024]{0,1:T(8,128)(2,1)} async-done(((bf16[768,512]{0,1:T(8,128)(2,1)}), bf16[768,1024]{0,1:T(8,128)(2,1)}) %all-gather.21.cloned.1.call-update) | async-done | bytes 1572880 | tf_op jit(solution)/shard_map/all_gather | solution.py:154
  274.6 5.0 %add_convert_fusion = bf16[768,1024]{1,0:T(8,128)(2,1)} fusion(f32[768,1024]{1,0:T(8,128)S(1)} %fusion.47, bf16[768,1024]{0,1:T(8,128)(2,1)} %all-gather.21.cloned.1.call-done, bf16[1024,1024]{1,0:T(8,128)(2,1)} %all-gather.23.cloned.1.call-done), kind=kOutput, calls=%fused_computation.16 | convolution fusion | flops 1612185600 | bytes 8388608 | tf_op jit(solution)/shard_map/dot_general | solution.py:153
  (87 shorter events, 22.8 us)
Async XLA Ops:
  6.5 107.6 %all-gather.9.cloned.1.call-start = ((), (), s32[]{:S(2)}) async-start(), calls=%async_computation.1 | async-start | bytes 4718592 | tf_op jit(solution)/shard_map/all_gather | solution.py:92
  7.3 118.7 %all-gather.11.cloned.1.call-start = ((), (), s32[]{:S(2)}) async-start(), calls=%async_computation.2 | async-start | bytes 2359296 | tf_op jit(solution)/shard_map/all_gather | solution.py:80
  8.0 145.6 %all-gather.19.cloned.1.call-start = ((), (), s32[]{:S(2)}) async-start(), calls=%async_computation.6 | async-start | bytes 2359296 | tf_op jit(solution)/shard_map/all_gather | solution.py:87
  8.7 160.7 %all-gather.17.cloned.1.call-start = ((), (), s32[]{:S(2)}) async-start(), calls=%async_computation.5 | async-start | bytes 2359296 | tf_op jit(solution)/shard_map/all_gather | solution.py:86
  10.0 103.4 %collective-permute-start.2 = (bf16[128,1]{0,1:T(2,128)(2,1)S(1)}, bf16[128,1]{0,1:T(2,128)(2,1)S(1)}, u32[]{:S(2)}, u32[]{:S(2)}) collective-permute-start(bf16[128,1]{0,1:T(2,128)(2,1)S(1)} %get-tuple-element.44), channel_id=1, source_target_pairs={{2,0},{4,2},{6,4},{8,6},{10,8},{12,10},{14,12},{3,1},{5,3},{7,5},{... | collective-permute-start | bytes 776 | tf_op jit(solution)/shard_map/ppermute | solution.py:22
  11.3 14.0 %copy-start.3 = (bf16[256,128]{1,0:T(8,128)(2,1)S(1)}, bf16[256,128]{1,0:T(8,128)(2,1)}, u32[]{:S(2)}) copy-start(bf16[256,128]{1,0:T(8,128)(2,1)} %param.18) | copy-start | bytes 196612
  11.3 102.1 %collective-permute-start.1 = (bf16[128,1]{0,1:T(2,128)(2,1)S(1)}, bf16[128,1]{0,1:T(2,128)(2,1)S(1)}, u32[]{:S(2)}, u32[]{:S(2)}) collective-permute-start(bf16[128,1]{0,1:T(2,128)(2,1)S(1)} %get-tuple-element.43), channel_id=1, source_target_pairs={{0,2},{2,4},{4,6},{6,8},{8,10},{10,12},{12,14},{1,3},{3,5},{5,7},{... | collective-permute-start | bytes 776 | tf_op jit(solution)/shard_map/ppermute | solution.py:20
  16.9 78.3 %copy-start.4 = (bf16[256,128]{1,0:T(8,128)(2,1)S(1)}, bf16[256,128]{1,0:T(8,128)(2,1)}, u32[]{:S(2)}) copy-start(bf16[256,128]{1,0:T(8,128)(2,1)} %param.17) | copy-start | bytes 196612
  16.9 96.3 %copy-start.8 = (f32[8]{0:T(128)S(1)}, f32[8]{0:T(128)}, u32[]{:S(2)}) copy-start(f32[8]{0:T(128)} %param.24) | copy-start | bytes 100
  16.9 142.3 %all-to-all-start = ((bf16[8,256,512]{2,1,0:T(8,128)(2,1)}), bf16[8,256,512]{2,1,0:T(8,128)(2,1)}, u32[]{:S(2)}, u32[]{:S(2)}) async-start(bf16[8,256,512]{2,1,0:T(8,128)(2,1)} %stack.2), calls=%async_computation | async-start | bytes 4194304 | tf_op jit(solution)/shard_map/all_to_all | solution.py:84
  23.4 93.5 %copy-start.6 = (f32[2048]{0:T(1024)S(1)}, f32[2048]{0:T(1024)}, u32[]{:S(2)}) copy-start(f32[2048]{0:T(1024)} %param.15) | copy-start | bytes 24580
  23.4 164.2 %all-gather.15.cloned.1.call-start = ((), (), s32[]{:S(2)}) async-start(), calls=%async_computation.4 | async-start | bytes 2359296 | tf_op jit(solution)/shard_map/all_gather | solution.py:88
  24.0 191.6 %all-gather.13.cloned.1.call-start = ((), (), s32[]{:S(2)}) async-start(), calls=%async_computation.3 | async-start | bytes 2359296 | tf_op jit(solution)/shard_map/all_gather | solution.py:151
  119.6 4.5 %collective-permute-start = (bf16[128,256]{0,1:T(8,128)(2,1)S(1)}, bf16[128,256]{0,1:T(8,128)(2,1)S(1)}, u32[]{:S(2)}, u32[]{:S(2)}) collective-permute-start(bf16[128,256]{0,1:T(8,128)(2,1)S(1)} %get-tuple-element.24), channel_id=1, source_target_pairs={{0,2},{2,4},{4,6},{6,8},{8,10},{10,12},{12,14},{1,3},{3,5},{5,7},{... | collective-permute-start | bytes 196616 | tf_op jit(solution)/shard_map/ppermute | solution.py:20
  121.9 4.0 %collective-permute-start.3 = (bf16[128,256]{0,1:T(8,128)(2,1)S(1)}, bf16[128,256]{0,1:T(8,128)(2,1)S(1)}, u32[]{:S(2)}, u32[]{:S(2)}) collective-permute-start(bf16[128,256]{0,1:T(8,128)(2,1)S(1)} %get-tuple-element.25), channel_id=1, source_target_pairs={{2,0},{4,2},{6,4},{8,6},{10,8},{12,10},{14,12},{3,1},{5,3},{7,5},{... | collective-permute-start | bytes 196616 | tf_op jit(solution)/shard_map/ppermute | solution.py:22
  139.5 12.2 %copy-start.5 = (f32[3,512]{1,0:T(4,128)S(1)}, f32[3,512]{1,0:T(4,128)}, u32[]{:S(2)}) copy-start(f32[3,512]{1,0:T(4,128)} %param.25) | copy-start | bytes 18436
  143.0 103.4 %all-gather.23.cloned.1.call-start = ((), (), s32[]{:S(2)}) async-start(), calls=%async_computation.8 | async-start | bytes 2359296 | tf_op jit(solution)/shard_map/all_gather | solution.py:89
  143.8 130.8 %all-gather.21.cloned.1.call-start = ((), (), s32[]{:S(2)}) async-start(), calls=%async_computation.7 | async-start | bytes 2359296 | tf_op jit(solution)/shard_map/all_gather | solution.py:154
  144.4 7.3 %collective-permute-start.5 = (bf16[1,1]{0,1:T(2,128)(2,1)}, bf16[1,1]{0,1:T(2,128)(2,1)}, u32[]{:S(2)}, u32[]{:S(2)}) collective-permute-start(bf16[1,1]{0,1:T(2,128)(2,1)} %bitcast.27), channel_id=1, source_target_pairs={{2,0},{4,2},{6,4},{8,6},{10,8},{12,10},{14,12},{3,1},{5,3},{7,5},{... | collective-permute-start | bytes 14 | tf_op jit(solution)/shard_map/ppermute | solution.py:22
  145.7 6.5 %collective-permute-start.4 = (bf16[1,1]{0,1:T(2,128)(2,1)}, bf16[1,1]{0,1:T(2,128)(2,1)}, u32[]{:S(2)}, u32[]{:S(2)}) collective-permute-start(bf16[1,1]{0,1:T(2,128)(2,1)} %bitcast.26), channel_id=1, source_target_pairs={{0,2},{2,4},{4,6},{6,8},{8,10},{10,12},{12,14},{1,3},{3,5},{5,7},{... | collective-permute-start | bytes 14 | tf_op jit(solution)/shard_map/ppermute | solution.py:20
  159.3 10.5 %copy-start.7 = (f32[512]{0:T(512)S(1)}, f32[512]{0:T(512)}, u32[]{:S(2)}) copy-start(f32[512]{0:T(512)} %param.26) | copy-start | bytes 6148
  163.2 6.1 %copy-start.2 = (bf16[768,512]{0,1:T(8,128)(2,1)}, bf16[768,512]{0,1:T(8,128)(2,1)S(1)}, u32[]{:S(2)}) copy-start(bf16[768,512]{0,1:T(8,128)(2,1)S(1)} %multiply_convert_fusion.1) | copy-start | bytes 2359300
  163.3 6.1 %collective-permute-start.7 = (bf16[1,512]{0,1:T(8,128)(2,1)S(1)}, bf16[1,512]{0,1:T(8,128)(2,1)}, u32[]{:S(2)}, u32[]{:S(2)}) collective-permute-start(bf16[1,512]{0,1:T(8,128)(2,1)S(1)} %get-tuple-element.13), channel_id=1, source_target_pairs={{2,0},{4,2},{6,4},{8,6},{10,8},{12,10},{14,12},{3,1},{5,3},{7,5},{... | collective-permute-start | bytes 3080 | tf_op jit(solution)/shard_map/ppermute | solution.py:22
  164.6 5.1 %collective-permute-start.6 = (bf16[1,512]{0,1:T(8,128)(2,1)S(1)}, bf16[1,512]{0,1:T(8,128)(2,1)}, u32[]{:S(2)}, u32[]{:S(2)}) collective-permute-start(bf16[1,512]{0,1:T(8,128)(2,1)S(1)} %get-tuple-element.12), channel_id=1, source_target_pairs={{0,2},{2,4},{4,6},{6,8},{8,10},{10,12},{12,14},{1,3},{3,5},{5,7},{... | collective-permute-start | bytes 3080 | tf_op jit(solution)/shard_map/ppermute | solution.py:20
  (2 other events, 8.6 us)
Sparse Core Ops, SparseCore 0:
  8.9 47.6 all-gather.8
  58.1 36.6 all-gather.10
  96.4 29.5 all-gather.18
  127.4 28.7 all-gather.16
  157.6 29.9 all-gather.14
  189.0 26.5 all-gather.12
  217.2 29.1 all-gather.22
  248.0 26.5 all-gather.20
